TPU v7x, 32 devices: a whole 2x2x4 slice. The times are simulated.
32 devices in a mesh: sp: 4 (over y, x), tp: 8 (over z, core).
Axes of the slice: x: 2, y: 2, z: 4, core: 2. Of those that a mesh axis runs over, the one named last changes fastest.
Arguments:
- inputs: bfloat16 [2, 2048, 4096], P(None, 'sp', 'tp'), may hold values from -16 to 16
- in_gain: float32 [4096], replicated, may hold values from 0.1 to 1.9
- key_weight: bfloat16 [4096, 2048], P(None, 'tp'), may hold values from -0.0014648438 to 0.0014648438
- value_weight: bfloat16 [4096, 4096], P(None, 'tp'), may hold values from -0.09375 to 0.09375
- decay_down: bfloat16 [4096, 32], replicated, may hold values from -0.09375 to 0.09375
- decay_up: bfloat16 [32, 2048], replicated, may hold values from -1 to 1
- decay_bias: float32 [2048], replicated, may hold values from 0 to 10
- new_query: bfloat16 [2, 2048], P(None, 'tp'), may hold values from -6 to 6
- out_gain: float32 [256], replicated, may hold values from 0.1 to 1.9
Outputs:
- cache: bfloat16 [2, 16, 128, 256], P(None, 'tp', 'sp')
- read: bfloat16 [2, 4096], P(None, 'tp')
All inputs are finite; a program needn't handle non-finite values.
Results may differ from a plain program's by a relative error of at most 0.0085.
Values may be sent and summed in bfloat16 or wider, within the bound.
A program may use at most 64 MiB of HBM per device.

v0:
```python
import jax
import jax.numpy as jnp
from jax import lax
from jax.sharding import PartitionSpec as P

D = 4096
DK = 128
DV = 256


def entering(value, axis, join, neutral):
    count, mine = (lax.axis_size(axis), lax.axis_index(axis))
    pieces = lax.all_gather(value, axis)
    pieces = pieces[::-1]
    mine = count - 1 - mine
    running = jnp.full_like(value, 0) + jnp.asarray(neutral, value.dtype)

    def step(position, running):
        longer = join(running, pieces[position])
        return jnp.where(position < mine, longer, running)

    return lax.fori_loop(0, count - 1, step, running)


def per_device(
    inputs, in_gain, key_weight, value_weight, decay_down, decay_up, decay_bias, new_query, out_gain
):
    seq_count, span_len, local_dim = inputs.shape
    tokens = seq_count * span_len
    key_cols = key_weight.shape[1]
    heads_here = key_cols // DK
    flat_rows = inputs.reshape(tokens, local_dim)
    tp_index = lax.axis_index("tp")
    contract = (((0,), (1,)), ((), ()))
    segment = lax.all_gather(flat_rows, "tp", axis=1, tiled=True)
    seg_scaled = (segment * in_gain).astype(jnp.bfloat16)
    seg_wide = segment.astype(jnp.float32)
    key_sum = lax.dot_general(key_weight, seg_scaled, contract, preferred_element_type=jnp.float32)
    value_sum = lax.dot_general(
        value_weight, seg_scaled, contract, preferred_element_type=jnp.float32
    )
    squares = jnp.sum(seg_wide * seg_wide, axis=1)
    low_part = jnp.dot(seg_scaled, decay_down, preferred_element_type=jnp.float32)
    inv_rms = lax.rsqrt(squares / D + 1e-06)
    key_rows = (key_sum * inv_rms).astype(jnp.bfloat16)
    value_rows = (value_sum * inv_rms).astype(jnp.bfloat16)
    low_rank = low_part * inv_rms[:, None]
    own_up = lax.dynamic_slice_in_dim(decay_up, tp_index * key_cols, key_cols, 1).astype(
        jnp.float32
    )
    own_bias = lax.dynamic_slice_in_dim(decay_bias, tp_index * key_cols, key_cols, 0)
    gate_pre = (
        lax.dot_general(own_up, low_rank, contract, precision=lax.Precision.HIGHEST)
        + own_bias[:, None]
    )
    log_decay = jax.nn.log_sigmoid(gate_pre) / 16.0
    blocks = log_decay.reshape(key_cols * seq_count, span_len)
    later_mask = (
        lax.broadcasted_iota(jnp.int32, (span_len, span_len), 0)
        > lax.broadcasted_iota(jnp.int32, (span_len, span_len), 1)
    ).astype(jnp.float32)
    suffix = jnp.dot(blocks, later_mask, precision=lax.Precision.HIGHEST).reshape(key_cols, tokens)
    block_total = jnp.sum(blocks, axis=1).reshape(heads_here, DK, seq_count).transpose(2, 0, 1)
    weighted = (key_rows.astype(jnp.float32) * jnp.exp(suffix)).astype(jnp.bfloat16)
    block_state = jnp.einsum(
        "hksp,hvsp->shkv",
        weighted.reshape(heads_here, DK, seq_count, span_len),
        value_rows.reshape(heads_here, DV, seq_count, span_len),
        preferred_element_type=jnp.float32,
    )
    later_sum = entering(block_total, "sp", jnp.add, jnp.zeros_like(block_total))
    terms = jnp.exp(later_sum)[..., None] * block_state
    state = lax.psum_scatter(terms, "sp", scatter_dimension=2, tiled=True)
    cache = state.astype(jnp.bfloat16)
    share_rows = DK // lax.axis_size("sp")
    queries = new_query.reshape(seq_count, heads_here, DK)
    query_part = lax.dynamic_slice_in_dim(queries, lax.axis_index("sp") * share_rows, share_rows, 2)
    partial_value = jnp.einsum(
        "shk,shkv->shv", query_part, cache, preferred_element_type=jnp.float32
    )
    readout = lax.psum(partial_value, "sp")
    normed = (
        readout * lax.rsqrt(jnp.mean(readout * readout, axis=-1, keepdims=True) + 1e-06) * out_gain
    )
    return (cache, normed.astype(jnp.bfloat16).reshape(seq_count, heads_here * DV))


def solution(mesh):
    in_specs = (
        P(None, "sp", "tp"),
        P(),
        P(None, "tp"),
        P(None, "tp"),
        P(),
        P(),
        P(),
        P(None, "tp"),
        P(),
    )
    out_specs = (P(None, "tp", "sp", None), P(None, "tp"))
    return jax.shard_map(
        per_device, mesh=mesh, in_specs=in_specs, out_specs=out_specs, check_vma=False
    )
```

profile of v0, /device:TPU:0, one launch (start us, length us, event | category | flops | bytes accessed | tf_op | source)
XLA Modules:
  0.0 183.7 jit_solution(15766181182852215187)
XLA Ops:
  7.2 0.7 all-gather.3.cloned.1.call-update
  8.0 0.8 dynamic_slice.17
  8.8 85.6 %all-gather.3.cloned.1.call-done = bf16[1024,4096]{1,0:T(8,128)(2,1)} async-done(((bf16[1024,512]{1,0:T(8,128)(2,1)}), bf16[1024,4096]{1,0:T(8,128)(2,1)}) %all-gather.3.cloned.1.call-update) | async-done | bytes 8388624 | tf_op jit(solution)/shard_map/all_gather | solution.py:35
  94.4 5.2 %fusion.1 = f32[1024]{0:T(1024)S(1)} fusion(bf16[1024,4096]{1,0:T(8,128)(2,1)} %all-gather.3.cloned.1.call-done), kind=kLoop, calls=%fused_computation.6 | loop fusion | flops 12581888 | bytes 8392704 | tf_op jit(solution)/shard_map/reduce_sum | solution.py:42
  99.7 0.5 copy-done.1
  100.2 2.6 %fusion.32 = f32[1024,32]{0,1:T(8,128)S(1)} fusion(bf16[4096,32]{0,1:T(8,128)(2,1)S(1)} %copy-done.5, bf16[1024,4096]{1,0:T(8,128)(2,1)S(1)} %copy-done.1, f32[4096]{0:T(1024)S(1)} %copy-done.6, f32[1024]{0:T(1024)S(1)} %add_rsqrt_fusion), kind=kOutput, calls=%fused_computation.23 | convolution fusion | flops 281051136 | bytes 8802304 | tf_op jit(solution)/shard_map/dot_general | solution.py:43
  102.8 3.0 %fusion.36 = f32[256,1024]{1,0:T(8,128)} fusion(f32[1024,32]{0,1:T(8,128)S(1)} %fusion.32, f32[256]{0:T(256)S(1)} %dynamic_slice.17, bf16[32,2048]{1,0:T(8,128)(2,1)} %param.16, s32[]{:T(128)S(6)} %select_n.33), kind=kOutput, calls=%fused_computation.25 | convolution fusion | flops 103284736 | bytes 1197060 | tf_op jit(solution)/shard_map/dot_general | solution.py:53
  105.8 1.4 reshape.50
  107.2 2.1 %convolution_exponential_fusion = f32[512,512]{1,0:T(8,128)} fusion(f32[512,512]{1,0:T(8,128)S(1)} %reshape.50), kind=kOutput, calls=%fused_computation.13 | convolution fusion | flops 1610874880 | bytes 2097152 | tf_op jit(solution)/shard_map/dot_general | solution.py:62
  109.3 0.1 reduce_sum.28
  109.4 1.6 exp.17
  111.0 1.4 copy.25
  112.4 10.0 %fusion.10 = bf16[512,1024]{0,1:T(8,128)(2,1)} fusion(bf16[4096,512]{1,0:T(8,128)(2,1)} %param.14, bf16[1024,4096]{1,0:T(8,128)(2,1)} %all-gather.3.cloned.1.call-done, f32[4096]{0:T(1024)S(1)} %copy-done.6, f32[1024]{0:T(1024)S(1)} %add_rsqrt_fusion), kind=kOutput, calls=%fused_computation.12 | convolution fusion | flops 4308598784 | bytes 13651968 | tf_op jit(solution)/shard_map/dot_general | solution.py:39
  122.5 1.3 reshape.53
  123.8 6.8 %fusion.29 = bf16[256,1024]{0,1:T(8,128)(2,1)} fusion(f32[256,1024]{0,1:T(8,128)} %copy.25, bf16[4096,256]{1,0:T(8,128)(2,1)S(1)} %copy-done, bf16[1024,4096]{1,0:T(8,128)(2,1)} %all-gather.3.cloned.1.call-done, f32[4096]{0:T(1024)S(1)} %copy-done.6, f32[1024]{0:T(1024)S(1)} %add_rsqrt_fusion), kind=kOutput, calls=%fused_computation.21 | convolution fusion | flops 2161377280 | bytes 12079104 | tf_op jit(solution)/shard_map/dot_general | solution.py:38
  130.6 2.0 %reshape.52 = bf16[2,128,2,512]{1,0,3,2:T(2,128)(2,1)} reshape(bf16[256,1024]{0,1:T(8,128)(2,1)} %fusion.29) | data formatting | bytes 1048576 | tf_op jit(solution)/shard_map/reshape | solution.py:67
  132.6 0.1 reshape.51
  132.8 8.1 %all-gather = f32[8,2,128]{2,1,0:T(2,128)S(1)} all-gather(f32[2,2,128]{2,1,0:T(2,128)S(1)} %copy.22), channel_id=2, replica_groups=mesh['sp'=4,'tp'=8] {'sp'}, dimensions={0}, use_global_device_ids=true | all-gather | bytes 10240 | tf_op jit(solution)/shard_map/all_gather | solution.py:13
  140.8 0.2 while.14
  141.0 2.2 %convolution_multiply_fusion = f32[2,2,128,256]{3,2,1,0:T(8,128)} fusion(bf16[2,256,2,512]{1,0,3,2:T(2,128)(2,1)S(1)} %reshape.53, bf16[2,128,2,512]{1,0,3,2:T(2,128)(2,1)} %reshape.52, f32[2,2,128]{2,1,0:T(2,128)S(1)} %exp.15), kind=kOutput, calls=%fused_computation.22 | convolution fusion | flops 134348800 | bytes 2099200 | tf_op jit(solution)/shard_map/hksp,hvsp->shkv/dot_general | solution.py:65
  143.4 22.7 %reduce-scatter.2.cloned.1.call-done = f32[2,2,32,256]{3,2,1,0:T(8,128)} async-done(((f32[2,2,128,256]{3,2,1,0:T(8,128)}), f32[2,2,32,256]{3,2,1,0:T(8,128)}) %reduce-scatter.2.cloned.1.call-update) | async-done | bytes 131088 | tf_op jit(solution)/shard_map/reduce_scatter | solution.py:73
  166.1 0.9 convert_element_type.42
  167.2 8.9 %psum.7 = f32[2,2,256]{2,1,0:T(2,128)S(1)} all-reduce(f32[2,2,256]{2,1,0:T(2,128)S(1)} %bitcast.38), channel_id=1, replica_groups=mesh['sp'=4,'tp'=8] {'sp'}, use_global_device_ids=true, to_apply=%region_5.6 | all-reduce | flops 1024 | bytes 8192 | tf_op jit(solution)/shard_map/psum | solution.py:81
  176.3 0.6 copy.31
  (35 shorter events, 0.7 us)
Async XLA Ops:
  7.2 116.6 %copy-start = (bf16[4096,256]{1,0:T(8,128)(2,1)S(1)}, bf16[4096,256]{1,0:T(8,128)(2,1)}, u32[]{:S(2)}) copy-start(bf16[4096,256]{1,0:T(8,128)(2,1)} %param.13) | copy-start | bytes 6291460
  7.2 92.5 %copy-start.6 = (f32[4096]{0:T(1024)S(1)}, f32[4096]{0:T(1024)}, u32[]{:S(2)}) copy-start(f32[4096]{0:T(1024)} %param.12) | copy-start | bytes 49156
  7.2 92.5 %copy-start.5 = (bf16[4096,32]{0,1:T(8,128)(2,1)S(1)}, bf16[4096,32]{0,1:T(8,128)(2,1)}, u32[]{:S(2)}) copy-start(bf16[4096,32]{0,1:T(8,128)(2,1)} %param.15) | copy-start | bytes 786436
  7.2 87.2 %all-gather.3.cloned.1.call-start = ((), (), s32[]{:S(2)}) async-start(), calls=%async_computation.1 | async-start | bytes 9437184 | tf_op jit(solution)/shard_map/all_gather | solution.py:35
  7.9 158.2 %reduce-scatter.2.cloned.1.call-start = ((), (), s32[]{:S(2)}) async-start(), calls=%async_computation.2 | async-start | bytes 655360 | tf_op jit(solution)/shard_map/reduce_scatter | solution.py:73
  94.4 5.8 %copy-start.1 = (bf16[1024,4096]{1,0:T(8,128)(2,1)S(1)}, bf16[1024,4096]{1,0:T(8,128)(2,1)}, u32[]{:S(2)}) copy-start(bf16[1024,4096]{1,0:T(8,128)(2,1)} %all-gather.3.cloned.1.call-done) | copy-start | bytes 25165828
  123.8 19.5 %copy-start.3 = (bf16[2,256]{1,0:T(2,128)(2,1)S(1)}, bf16[2,256]{1,0:T(2,128)(2,1)}, u32[]{:S(2)}) copy-start(bf16[2,256]{1,0:T(2,128)(2,1)} %param.18) | copy-start | bytes 3076
  123.8 52.4 %copy-start.4 = (f32[256]{0:T(256)S(1)}, f32[256]{0:T(256)}, u32[]{:S(2)}) copy-start(f32[256]{0:T(256)} %param.19) | copy-start | bytes 3076
  167.0 9.8 %copy-start.2 = (bf16[2,2,32,256]{3,2,1,0:T(8,128)(2,1)}, bf16[2,2,32,256]{3,2,1,0:T(8,128)(2,1)S(1)}, u32[]{:S(2)}) copy-start(bf16[2,2,32,256]{3,2,1,0:T(8,128)(2,1)S(1)} %convert_element_type.42) | copy-start | bytes 196612
Sparse Core Ops, SparseCore 0:
  9.6 84.7 all-gather.2
  143.4 22.6 reduce-scatter.1
where the time goes:
time: 184 us
  waiting for transfers between devices  109 us (59%)
  matrix products  26.9 us (15%)
  blocking collectives  17 us (9%)
  between operations  14.2 us (8%)
  local copies, waits for them, and re-layouts  9.93 us (5%)
  other arithmetic  6.51 us (4%)
    all_gather x1, waiting for transfers between devices, per_device(): segment = lax.all_gather(flat_rows, 'tp', axis=1, tiled=True)  85.6 us
    reduce_scatter x1, waiting for transfers between devices, per_device(): state = lax.psum_scatter(terms, 'sp', scatter_dimension=2, tiled=True)  22.7 us
    dot_general x1, matrix products, per_device(): lax.dot_general(value_weight, seg_scaled, contract, preferred_element_typ...  10 us
    psum x1, blocking collectives, per_device(): readout = lax.psum(partial_value, 'sp')  8.92 us
    all_gather x1, blocking collectives, entering(): pieces = lax.all_gather(value, axis)  8.05 us
    dot_general x1, matrix products, per_device(): lax.dot_general(key_weight, seg_scaled, contract, preferred_element_type=...  6.76 us
    reduce_sum x1, other arithmetic, per_device(): squares = jnp.sum(seg_wide * seg_wide, axis=1)  5.22 us
  transfers between devices with their start and end apart: 2, of which 2 were waited for; matrix products, arithmetic and copies ran while one was open for 0% of the time, Pallas kernels for 0%

commit v1 on v0

v1 whole, which is shorter than its diff:
```python
import functools

import jax
import jax.numpy as jnp
from jax import lax
from jax.experimental import pallas as pl
from jax.experimental.pallas import tpu as pltpu
from jax.sharding import PartitionSpec as P

DK = 128
DV = 256
CHUNK = 256
AHEAD = 2
MESH = pl.DeviceIdType.MESH
F32 = jnp.float32
BF16 = jnp.bfloat16


def split3(value):
    high = value.astype(BF16)
    rest = value - high.astype(F32)
    middle = rest.astype(BF16)
    low = (rest - middle.astype(F32)).astype(BF16)
    return high, middle, low


def kernel(
    n_sp,
    n_z,
    x_ref,
    gain_ref,
    wk_hbm,
    wv_hbm,
    wd_hbm,
    up_hbm,
    bias_hbm,
    query_ref,
    out_gain_ref,
    cache_ref,
    read_ref,
    xbuf,
    wk,
    wv,
    wd,
    up,
    bias,
    acc_k,
    acc_v,
    acc_l,
    acc_s,
    state,
    carry,
    tots,
    terms,
    landed,
    reads,
    load_sem,
    own_sem,
    line_send,
    pair_send,
    recv,
    tot_send,
    tot_recv,
    term_send,
    term_recv,
    read_send,
    read_recv,
):
    seqs, span, feats = x_ref.shape
    per_seq = span // CHUNK
    chunks = seqs * per_seq
    heads = wk_hbm.shape[1] // DK
    share = DK // n_sp
    model = n_z * 2 * feats
    sp = lax.axis_index("sp")
    tp = lax.axis_index("tp")
    z = tp // 2
    c = lax.rem(tp, 2)
    key_cols = heads * DK

    first = pl.multiple_of(tp * key_cols, key_cols)
    loads = [
        pltpu.make_async_copy(wk_hbm, wk, load_sem.at[0]),
        pltpu.make_async_copy(wv_hbm, wv, load_sem.at[1]),
        pltpu.make_async_copy(wd_hbm, wd, load_sem.at[2]),
        pltpu.make_async_copy(up_hbm.at[:, pl.ds(first, key_cols)], up, load_sem.at[3]),
        pltpu.make_async_copy(bias_hbm.at[:, pl.ds(first, key_cols)], bias, load_sem.at[4]),
    ]

    def chunk_rows(j):
        seq = j // per_seq
        start = (per_seq - 1 - lax.rem(j, per_seq)) * CHUNK
        return seq, pl.multiple_of(start, CHUNK)

    def own_copy(j):
        seq, start = chunk_rows(j)
        return pltpu.make_async_copy(
            x_ref.at[seq, pl.ds(start, CHUNK), :], xbuf.at[j, z, c], own_sem.at[j]
        )

    def line_copy(j, zz, way):
        return pltpu.make_async_remote_copy(
            src_ref=xbuf.at[j, zz, c],
            dst_ref=xbuf.at[j, zz, c],
            send_sem=line_send.at[(way + 1) // 2, j, zz],
            recv_sem=recv.at[j, zz, c],
            device_id={"tp": tp + 2 * way},
            device_id_type=MESH,
        )

    def pair_copy(j, zz, cc):
        return pltpu.make_async_remote_copy(
            src_ref=xbuf.at[j, zz, cc],
            dst_ref=xbuf.at[j, zz, cc],
            send_sem=pair_send.at[j, zz],
            recv_sem=recv.at[j, zz, cc],
            device_id={"tp": tp + 1 - 2 * c},
            device_id_type=MESH,
        )

    for j in range(chunks):
        own_copy(j).start()

    barrier = pltpu.get_barrier_semaphore()
    for way in (-1, 1):
        there = z + way

        @pl.when((there >= 0) & (there < n_z))
        def _():
            pl.semaphore_signal(
                barrier, inc=1, device_id={"tp": tp + 2 * way}, device_id_type=MESH
            )

    pl.semaphore_signal(barrier, inc=1, device_id={"tp": tp + 1 - 2 * c}, device_id_type=MESH)
    for off in range(1, n_sp):
        pl.semaphore_signal(
            barrier, inc=1, device_id={"sp": lax.rem(sp + off, n_sp)}, device_id_type=MESH
        )
    lines = jnp.where(z > 0, 1, 0) + jnp.where(z < n_z - 1, 1, 0)
    pl.semaphore_wait(barrier, lines + n_sp)

    def send_own(j):
        own_copy(j).wait()
        for way in (-1, 1):
            there = z + way

            @pl.when((there >= 0) & (there < n_z))
            def _():
                line_copy(j, z, way).start()

        pair_copy(j, z, c).start()

    for j in range(min(AHEAD, chunks)):
        send_own(j)
    for load in loads:
        load.start()
    for load in loads:
        load.wait()

    def clear_chunk():
        acc_k[...] = jnp.zeros_like(acc_k)
        acc_v[...] = jnp.zeros_like(acc_v)
        acc_l[...] = jnp.zeros_like(acc_l)
        acc_s[...] = jnp.zeros_like(acc_s)

    def add_shard(j, zz, cc):
        slot = zz * 2 + cc
        wide = xbuf[j, zz, cc].astype(F32)
        scaled = (wide * gain_ref[slot]).astype(BF16)
        rows = pl.ds(pl.multiple_of(slot * feats, feats), feats)
        acc_k[...] += jnp.dot(scaled, wk[rows, :], preferred_element_type=F32)
        acc_v[...] += jnp.dot(scaled, wv[rows, :], preferred_element_type=F32)
        acc_l[...] += jnp.dot(scaled, wd[rows, :], preferred_element_type=F32)
        square = wide * wide
        total = square[:, 0:128]
        for lane in range(128, feats, 128):
            total = total + square[:, lane : lane + 128]
        acc_s[...] += total

    def gather_step(j, i):
        away = (i + 1) // 2
        way = 1 - 2 * lax.rem(i, 2)
        zz = z + way * away

        @pl.when((zz >= 0) & (zz < n_z))
        def _():
            @pl.when(i > 0)
            def _():
                line_copy(j, zz, 1).wait_recv()
                onward = z - way

                @pl.when((onward >= 0) & (onward < n_z))
                def _():
                    line_copy(j, zz, -way).start()

                pair_copy(j, zz, c).start()

            add_shard(j, zz, c)
            pair_copy(j, zz, 1 - c).wait_recv()
            add_shard(j, zz, 1 - c)

    def finish_chunk(j):
        seq = j // per_seq

        @pl.when(lax.rem(j, per_seq) == 0)
        def _():
            carry[...] = jnp.zeros_like(carry)
            state[seq] = jnp.zeros(state.shape[1:], F32)

        inv_rms = lax.rsqrt(jnp.sum(acc_s[...], axis=1, keepdims=True) / model + 1e-06)
        low_rank = acc_l[...] * inv_rms
        gate = (
            jnp.dot(
                low_rank,
                up[...].astype(F32),
                precision=lax.Precision.HIGHEST,
                preferred_element_type=F32,
            )
            + bias[...]
        )
        log_decay = (jnp.minimum(gate, 0.0) - jnp.log1p(jnp.exp(-jnp.abs(gate)))) / 16.0
        later = (
            lax.broadcasted_iota(jnp.int32, (CHUNK, CHUNK), 1)
            > lax.broadcasted_iota(jnp.int32, (CHUNK, CHUNK), 0)
        ).astype(BF16)
        suffix = carry[...]
        for piece in split3(log_decay):
            suffix = suffix + jnp.dot(later, piece, preferred_element_type=F32)
        carry[...] = carry[...] + jnp.sum(log_decay, axis=0, keepdims=True)
        keys = (acc_k[...] * inv_rms).astype(BF16).astype(F32)
        weighted = keys * jnp.exp(suffix)
        values = (acc_v[...] * inv_rms).astype(BF16)
        for h in range(heads):
            part = weighted[:, h * DK : (h + 1) * DK].T.astype(BF16)
            rows = pl.ds(h * DK, DK)
            state[seq, rows, :] = state[seq, rows, :] + jnp.dot(
                part, values[:, h * DV : (h + 1) * DV], preferred_element_type=F32
            )

    peers = [lax.rem(sp + off, n_sp) for off in range(1, n_sp)]

    def tot_copy(seq, peer, slot):
        return pltpu.make_async_remote_copy(
            src_ref=tots.at[seq, sp],
            dst_ref=tots.at[seq, slot],
            send_sem=tot_send.at[seq, peer],
            recv_sem=tot_recv.at[seq, slot],
            device_id={"sp": peer},
            device_id_type=MESH,
        )

    def term_copy(seq, peer, slot):
        return pltpu.make_async_remote_copy(
            src_ref=terms.at[seq, peer],
            dst_ref=landed.at[seq, slot],
            send_sem=term_send.at[seq, peer],
            recv_sem=term_recv.at[seq, slot],
            device_id={"sp": peer},
            device_id_type=MESH,
        )

    def read_copy(seq, peer, slot):
        return pltpu.make_async_remote_copy(
            src_ref=reads.at[seq, sp],
            dst_ref=reads.at[seq, slot],
            send_sem=read_send.at[seq, peer],
            recv_sem=read_recv.at[seq, slot],
            device_id={"sp": peer},
            device_id_type=MESH,
        )

    def send_total(seq):
        tots[seq, sp] = carry[...]
        for peer in peers:
            tot_copy(seq, peer, sp).start()

    def send_terms(seq):
        for peer in peers:
            tot_copy(seq, peer, peer).wait_recv()
        after = jnp.zeros((1, key_cols), F32)
        for p in range(n_sp):
            after = after + jnp.where(p > sp, tots[seq, p], 0.0)
        factor = jnp.broadcast_to(jnp.exp(after), (128, key_cols)).T
        for h in range(heads):
            for p in range(n_sp):
                row = h * DK + p * share
                scale = factor[row : row + share, :]
                for lane in range(0, DV, 128):
                    terms[seq, p, h, :, lane : lane + 128] = (
                        state[seq, row : row + share, lane : lane + 128] * scale
                    )
        for peer in peers:
            term_copy(seq, peer, sp).start()

    def send_reads(seq):
        total = terms[seq, sp]
        for peer in peers:
            term_copy(seq, peer, peer).wait_recv()
            total = total + landed[seq, peer]
        cache = total.astype(BF16)
        cache_ref[seq] = cache
        wide = cache.astype(F32)
        chosen = (
            lax.broadcasted_iota(jnp.int32, (share, DK), 0) + sp * share
            == lax.broadcasted_iota(jnp.int32, (share, DK), 1)
        )
        for h in range(heads):
            queries = query_ref[seq : seq + 1, h * DK : (h + 1) * DK].astype(F32)
            column = jnp.sum(jnp.where(chosen, queries, 0.0), axis=1, keepdims=True)
            reads[seq, sp, h : h + 1, :] = jnp.sum(column * wide[h], axis=0, keepdims=True)
        for peer in peers:
            read_copy(seq, peer, sp).start()

    def give_read(seq):
        for peer in peers:
            read_copy(seq, peer, peer).wait_recv()
        readout = reads[seq, 0]
        for p in range(1, n_sp):
            readout = readout + reads[seq, p]
        mean = jnp.mean(readout * readout, axis=-1, keepdims=True)
        normed = (readout * lax.rsqrt(mean + 1e-06) * out_gain_ref[...]).astype(BF16)
        for h in range(heads):
            read_ref[seq : seq + 1, h * DV : (h + 1) * DV] = normed[h : h + 1, :]

    def chunk_step(j, _):
        @pl.when(j + AHEAD < chunks)
        def _():
            send_own(j + AHEAD)

        clear_chunk()

        def inner(i, _):
            gather_step(j, i)
            return 0

        lax.fori_loop(0, 2 * n_z - 1, inner, 0)
        finish_chunk(j)
        for seq in range(seqs):
            done = (seq + 1) * per_seq - 1

            @pl.when(j == done)
            def _():
                send_total(seq)

            if seq < seqs - 1:

                @pl.when(j == done + 1)
                def _():
                    send_terms(seq)

        return 0

    lax.fori_loop(0, chunks, chunk_step, 0)
    for seq in range(seqs - 1):
        send_reads(seq)
    send_terms(seqs - 1)
    send_reads(seqs - 1)
    for seq in range(seqs):
        give_read(seq)

    def drain(j, _):
        pair_copy(j, z, c).wait_send()
        for way in (-1, 1):
            there = z + way

            @pl.when((there >= 0) & (there < n_z))
            def _():
                line_copy(j, z, way).wait_send()

        def inner(i, _):
            away = (i + 1) // 2
            way = 1 - 2 * lax.rem(i, 2)
            zz = z + way * away

            @pl.when((zz >= 0) & (zz < n_z))
            def _():
                onward = z - way

                @pl.when((onward >= 0) & (onward < n_z))
                def _():
                    line_copy(j, zz, -way).wait_send()

                pair_copy(j, zz, c).wait_send()

            return 0

        lax.fori_loop(1, 2 * n_z - 1, inner, 0)
        return 0

    lax.fori_loop(0, chunks, drain, 0)
    for seq in range(seqs):
        for peer in peers:
            tot_copy(seq, peer, sp).wait_send()
            term_copy(seq, peer, sp).wait_send()
            read_copy(seq, peer, sp).wait_send()


def per_device(
    n_sp,
    n_z,
    inputs,
    in_gain,
    key_weight,
    value_weight,
    decay_down,
    decay_up,
    decay_bias,
    new_query,
    out_gain,
):
    seqs, span, feats = inputs.shape
    model, key_cols = key_weight.shape
    value_cols = value_weight.shape[1]
    rank = decay_down.shape[1]
    heads = key_cols // DK
    chunks = seqs * (span // CHUNK)
    share = DK // n_sp
    vmem = pl.BlockSpec(memory_space=pltpu.VMEM)
    hbm = pl.BlockSpec(memory_space=pl.ANY)
    dma = pltpu.SemaphoreType.DMA
    return pl.pallas_call(
        functools.partial(kernel, n_sp, n_z),
        out_shape=(
            jax.ShapeDtypeStruct((seqs, heads, share, DV), BF16),
            jax.ShapeDtypeStruct((seqs, heads * DV), BF16),
        ),
        in_specs=[hbm, vmem, hbm, hbm, hbm, hbm, hbm, vmem, vmem],
        out_specs=(vmem, vmem),
        scratch_shapes=[
            pltpu.VMEM((chunks, n_z, 2, CHUNK, feats), BF16),
            pltpu.VMEM((model, key_cols), BF16),
            pltpu.VMEM((model, value_cols), BF16),
            pltpu.VMEM((model, rank), BF16),
            pltpu.VMEM((rank, key_cols), BF16),
            pltpu.VMEM((1, key_cols), F32),
            pltpu.VMEM((CHUNK, key_cols), F32),
            pltpu.VMEM((CHUNK, value_cols), F32),
            pltpu.VMEM((CHUNK, rank), F32),
            pltpu.VMEM((CHUNK, 128), F32),
            pltpu.VMEM((seqs, key_cols, DV), F32),
            pltpu.VMEM((1, key_cols), F32),
            pltpu.VMEM((seqs, n_sp, 1, key_cols), F32),
            pltpu.VMEM((seqs, n_sp, heads, share, DV), F32),
            pltpu.VMEM((seqs, n_sp, heads, share, DV), F32),
            pltpu.VMEM((seqs, n_sp, heads, DV), F32),
            dma((5,)),
            dma((chunks,)),
            dma((2, chunks, n_z)),
            dma((chunks, n_z)),
            dma((chunks, n_z, 2)),
            dma((seqs, n_sp)),
            dma((seqs, n_sp)),
            dma((seqs, n_sp)),
            dma((seqs, n_sp)),
            dma((seqs, n_sp)),
            dma((seqs, n_sp)),
        ],
        compiler_params=pltpu.CompilerParams(
            collective_id=0, has_side_effects=True, vmem_limit_bytes=60 * 1024 * 1024
        ),
    )(
        inputs,
        in_gain.reshape(2 * n_z, 1, feats),
        key_weight,
        value_weight,
        decay_down,
        decay_up,
        decay_bias.reshape(1, -1),
        new_query,
        out_gain.reshape(1, -1),
    )


def solution(mesh):
    in_specs = (
        P(None, "sp", "tp"),
        P(),
        P(None, "tp"),
        P(None, "tp"),
        P(),
        P(),
        P(),
        P(None, "tp"),
        P(),
    )
    out_specs = (P(None, "tp", "sp", None), P(None, "tp"))
    return jax.shard_map(
        functools.partial(per_device, mesh.shape["sp"], mesh.shape["tp"] // 2),
        mesh=mesh,
        in_specs=in_specs,
        out_specs=out_specs,
        check_vma=False,
    )
```

time: 184 us -> 101 us (0.55)
  waiting for transfers between devices: 109 us -> 0 us
  Pallas kernels: 0 us -> 94.7 us
  matrix products: 26.9 us -> 0 us
  blocking collectives: 17 us -> 0 us
  between operations: 14.2 us -> 0.64 us
  other arithmetic: 6.51 us -> 0 us
  local copies, waits for them, and re-layouts: 9.93 us -> 5.02 us
    pallas_call x0 -> x1, Pallas kernels: none -> 94.7 us  [per_device(): pl.pallas_call(functools.partial(kernel, n_sp, n_z), out_shape=(jax.Shape...]
    all_gather x1 -> x0, waiting for transfers between devices: 85.6 us -> none  [per_device(): segment = lax.all_gather(flat_rows, 'tp', axis=1, tiled=True)]
    dot_general x7 -> x0, matrix products: 26.9 us -> none  [the longest x1 10 us: per_device(): lax.dot_general(value_weight, seg_scaled, contract, preferred_element_typ...]
    reduce_scatter x1 -> x0, waiting for transfers between devices: 22.7 us -> none  [per_device(): state = lax.psum_scatter(terms, 'sp', scatter_dimension=2, tiled=True)]
    psum x1 -> x0, blocking collectives: 8.92 us -> none  [per_device(): readout = lax.psum(partial_value, 'sp')]
    all_gather x1 -> x0, blocking collectives: 8.05 us -> none  [entering(): pieces = lax.all_gather(value, axis)]
    reduce_sum x3 -> x0, other arithmetic: 5.46 us -> none  [the longest x1 5.22 us: per_device(): squares = jnp.sum(seg_wide * seg_wide, axis=1)]
    reshape x5 -> x0, local copies, waits for them, and re-layouts: 4.85 us -> none  [the longest x1 1.95 us: per_device(): weighted.reshape(heads_here, DK, seq_count, span_len)]
  transfers between devices with their start and end apart: 2 -> 0, of which waited for: 2 -> 0; matrix products, arithmetic and copies ran while one was open for 0% -> 0% of each run, Pallas kernels for 0% -> 0%
where the time goes in v1:
time: 101 us; the launch traced here: 100 us
  Pallas kernels  94.7 us (94%)
  local copies, waits for them, and re-layouts  5.02 us (5%)
    pallas_call x1, Pallas kernels, per_device(): pl.pallas_call(functools.partial(kernel, n_sp, n_z), out_shape=(jax.Shape...  94.7 us
    unnamed x3, local copies, waits for them, and re-layouts  5.02 us

profile of v1, /device:TPU:0, one launch (start us, length us, event | category | flops | bytes accessed | tf_op | source)
XLA Modules:
  0.0 100.3 jit_solution(7445490174417022928)
XLA Ops:
  0.6 2.3 %copy.11.wd_hbm = bf16[4096,32]{1,0:T(8,128)(2,1)} copy(bf16[4096,32]{0,1:T(8,128)(2,1)} %param.13) | data formatting | bytes 524288 | tf_op args[4]
  2.9 94.7 %shard_map.104 = (bf16[2,2,32,256]{3,2,1,0:T(8,128)(2,1)}, bf16[2,512]{1,0:T(2,128)(2,1)}) custom-call(bf16[2,512,512]{2,1,0:T(8,128)(2,1)} %x_ref.1, f32[8,1,512]{2,1,0:T(1,128)} %bitcast.3, bf16[4096,256]{1,0:T(8,128)(2,1)} %wk_hbm.1, bf16[4096,512]{1,0:T(8,128)(2,1)} %wv_hbm.1, bf16[4096,32]{1,0:T(8,128)(2,1)} %copy.11.wd_hbm, bf16[32,2048]{1,0:T(8,128)(2,1)} %up_hbm.1, ...), custom_call_target="tpu_custom_call" | custom-call | tf_op jit(solution)/shard_map/pallas_call | solution.py:421
  97.6 1.5 %copy.14 = bf16[2,2,32,256]{3,2,1,0:T(8,128)(2,1)} copy(bf16[2,2,32,256]{3,2,1,0:T(8,128)(2,1)} %get-tuple-element.4) | data formatting | bytes 131072
  99.1 1.3 %copy.15 = bf16[2,512]{1,0:T(2,128)(2,1)} copy(bf16[2,512]{1,0:T(2,128)(2,1)} %get-tuple-element.5) | data formatting | bytes 4096

commit v2 on v1

--- a/solution.py
+++ b/solution.py
@@ -9,8 +9,8 @@
 
 DK = 128
 DV = 256
-CHUNK = 256
-AHEAD = 2
+CHUNK = 128
+AHEAD = 4
 MESH = pl.DeviceIdType.MESH
 F32 = jnp.float32
 BF16 = jnp.bfloat16
@@ -35,9 +35,8 @@
     up_hbm,
     bias_hbm,
     query_ref,
-    out_gain_ref,
     cache_ref,
-    read_ref,
+    parts_ref,
     xbuf,
     wk,
     wv,
@@ -170,7 +169,9 @@
         rows = pl.ds(pl.multiple_of(slot * feats, feats), feats)
         acc_k[...] += jnp.dot(scaled, wk[rows, :], preferred_element_type=F32)
         acc_v[...] += jnp.dot(scaled, wv[rows, :], preferred_element_type=F32)
-        acc_l[...] += jnp.dot(scaled, wd[rows, :], preferred_element_type=F32)
+        acc_l[...] += lax.dot_general(
+            scaled, wd[:, rows], (((1,), (1,)), ((), ())), preferred_element_type=F32
+        )
         square = wide * wide
         total = square[:, 0:128]
         for lane in range(128, feats, 128):
@@ -227,6 +228,12 @@
         for piece in split3(log_decay):
             suffix = suffix + jnp.dot(later, piece, preferred_element_type=F32)
         carry[...] = carry[...] + jnp.sum(log_decay, axis=0, keepdims=True)
+        last = lax.rem(j, per_seq) == per_seq - 1
+
+        @pl.when(last)
+        def _():
+            send_total(seq)
+
         keys = (acc_k[...] * inv_rms).astype(BF16).astype(F32)
         weighted = keys * jnp.exp(suffix)
         values = (acc_v[...] * inv_rms).astype(BF16)
@@ -237,6 +244,10 @@
                 part, values[:, h * DV : (h + 1) * DV], preferred_element_type=F32
             )
 
+        @pl.when(last)
+        def _():
+            send_terms(seq)
+
     peers = [lax.rem(sp + off, n_sp) for off in range(1, n_sp)]
 
     def tot_copy(seq, peer, slot):
@@ -275,52 +286,57 @@
             tot_copy(seq, peer, sp).start()
 
     def send_terms(seq):
-        for peer in peers:
-            tot_copy(seq, peer, peer).wait_recv()
-        after = jnp.zeros((1, key_cols), F32)
-        for p in range(n_sp):
-            after = after + jnp.where(p > sp, tots[seq, p], 0.0)
-        factor = jnp.broadcast_to(jnp.exp(after), (128, key_cols)).T
         for h in range(heads):
             for p in range(n_sp):
                 row = h * DK + p * share
-                scale = factor[row : row + share, :]
-                for lane in range(0, DV, 128):
-                    terms[seq, p, h, :, lane : lane + 128] = (
-                        state[seq, row : row + share, lane : lane + 128] * scale
-                    )
+                terms[seq, p, h] = state[seq, row : row + share, :].astype(BF16)
         for peer in peers:
             term_copy(seq, peer, sp).start()
 
     def send_reads(seq):
-        total = terms[seq, sp]
-        for peer in peers:
-            term_copy(seq, peer, peer).wait_recv()
-            total = total + landed[seq, peer]
-        cache = total.astype(BF16)
-        cache_ref[seq] = cache
-        wide = cache.astype(F32)
         chosen = (
             lax.broadcasted_iota(jnp.int32, (share, DK), 0) + sp * share
             == lax.broadcasted_iota(jnp.int32, (share, DK), 1)
         )
+
+        def column(row):
+            return jnp.sum(jnp.where(chosen, row, 0.0), axis=1, keepdims=True)
+
+        for peer in peers:
+            tot_copy(seq, peer, peer).wait_recv()
+        after = jnp.zeros((1, key_cols), F32)
+        factors = [None] * n_sp
+        for p in reversed(range(n_sp)):
+            decay = jnp.exp(after)
+            factors[p] = [column(decay[:, h * DK : (h + 1) * DK]) for h in range(heads)]
+            after = after + tots[seq, p]
+        for peer in peers:
+            term_copy(seq, peer, peer).wait_recv()
+        own = [
+            state[seq, pl.ds(pl.multiple_of(h * DK + sp * share, share), share), :]
+            for h in range(heads)
+        ]
+        sums = []
         for h in range(heads):
+            total = jnp.zeros((share, DV), F32)
+            for p in range(n_sp):
+                block = jnp.where(p == sp, own[h], landed[seq, p, h].astype(F32))
+                total = total + factors[p][h] * block
+            sums.append(total)
+        for h in range(heads):
+            cache = sums[h].astype(BF16)
+            cache_ref[seq, h] = cache
             queries = query_ref[seq : seq + 1, h * DK : (h + 1) * DK].astype(F32)
-            column = jnp.sum(jnp.where(chosen, queries, 0.0), axis=1, keepdims=True)
-            reads[seq, sp, h : h + 1, :] = jnp.sum(column * wide[h], axis=0, keepdims=True)
+            reads[seq, sp, h : h + 1, :] = jnp.sum(
+                column(queries) * cache.astype(F32), axis=0, keepdims=True
+            )
         for peer in peers:
             read_copy(seq, peer, sp).start()
 
     def give_read(seq):
         for peer in peers:
             read_copy(seq, peer, peer).wait_recv()
-        readout = reads[seq, 0]
-        for p in range(1, n_sp):
-            readout = readout + reads[seq, p]
-        mean = jnp.mean(readout * readout, axis=-1, keepdims=True)
-        normed = (readout * lax.rsqrt(mean + 1e-06) * out_gain_ref[...]).astype(BF16)
-        for h in range(heads):
-            read_ref[seq : seq + 1, h * DV : (h + 1) * DV] = normed[h : h + 1, :]
+        parts_ref[seq] = reads[seq]
 
     def chunk_step(j, _):
         @pl.when(j + AHEAD < chunks)
@@ -335,29 +351,12 @@
 
         lax.fori_loop(0, 2 * n_z - 1, inner, 0)
         finish_chunk(j)
-        for seq in range(seqs):
-            done = (seq + 1) * per_seq - 1
-
-            @pl.when(j == done)
-            def _():
-                send_total(seq)
-
-            if seq < seqs - 1:
-
-                @pl.when(j == done + 1)
-                def _():
-                    send_terms(seq)
-
         return 0
 
-    lax.fori_loop(0, chunks, chunk_step, 0)
+    lax.fori_loop(0, chunks - 1, chunk_step, 0)
     for seq in range(seqs - 1):
         send_reads(seq)
-    send_terms(seqs - 1)
-    send_reads(seqs - 1)
-    for seq in range(seqs):
-        give_read(seq)
-
+    chunk_step(chunks - 1, 0)
     def drain(j, _):
         pair_copy(j, z, c).wait_send()
         for way in (-1, 1):
@@ -388,11 +387,27 @@
         return 0
 
     lax.fori_loop(0, chunks, drain, 0)
+    send_reads(seqs - 1)
+    for seq in range(seqs):
+        give_read(seq)
     for seq in range(seqs):
         for peer in peers:
             tot_copy(seq, peer, sp).wait_send()
             term_copy(seq, peer, sp).wait_send()
             read_copy(seq, peer, sp).wait_send()
+
+
+def norm_kernel(cache_in, parts_ref, gain_ref, cache_ref, read_ref):
+    cache_ref[...] = cache_in[...]
+    seqs, n_sp, heads, _ = parts_ref.shape
+    for seq in range(seqs):
+        readout = parts_ref[seq, 0]
+        for p in range(1, n_sp):
+            readout = readout + parts_ref[seq, p]
+        mean = jnp.mean(readout * readout, axis=-1, keepdims=True)
+        normed = (readout * lax.rsqrt(mean + 1e-06) * gain_ref[...]).astype(BF16)
+        for h in range(heads):
+            read_ref[seq : seq + 1, h * DV : (h + 1) * DV] = normed[h : h + 1, :]
 
 
 def per_device(
@@ -418,19 +433,19 @@
     vmem = pl.BlockSpec(memory_space=pltpu.VMEM)
     hbm = pl.BlockSpec(memory_space=pl.ANY)
     dma = pltpu.SemaphoreType.DMA
-    return pl.pallas_call(
+    cache, parts = pl.pallas_call(
         functools.partial(kernel, n_sp, n_z),
         out_shape=(
             jax.ShapeDtypeStruct((seqs, heads, share, DV), BF16),
-            jax.ShapeDtypeStruct((seqs, heads * DV), BF16),
+            jax.ShapeDtypeStruct((seqs, n_sp, heads, DV), F32),
         ),
-        in_specs=[hbm, vmem, hbm, hbm, hbm, hbm, hbm, vmem, vmem],
+        in_specs=[hbm, vmem, hbm, hbm, hbm, hbm, hbm, vmem],
         out_specs=(vmem, vmem),
         scratch_shapes=[
             pltpu.VMEM((chunks, n_z, 2, CHUNK, feats), BF16),
             pltpu.VMEM((model, key_cols), BF16),
             pltpu.VMEM((model, value_cols), BF16),
-            pltpu.VMEM((model, rank), BF16),
+            pltpu.VMEM((rank, model), BF16),
             pltpu.VMEM((rank, key_cols), BF16),
             pltpu.VMEM((1, key_cols), F32),
             pltpu.VMEM((CHUNK, key_cols), F32),
@@ -440,8 +455,8 @@
             pltpu.VMEM((seqs, key_cols, DV), F32),
             pltpu.VMEM((1, key_cols), F32),
             pltpu.VMEM((seqs, n_sp, 1, key_cols), F32),
-            pltpu.VMEM((seqs, n_sp, heads, share, DV), F32),
-            pltpu.VMEM((seqs, n_sp, heads, share, DV), F32),
+            pltpu.VMEM((seqs, n_sp, heads, share, DV), BF16),
+            pltpu.VMEM((seqs, n_sp, heads, share, DV), BF16),
             pltpu.VMEM((seqs, n_sp, heads, DV), F32),
             dma((5,)),
             dma((chunks,)),
@@ -463,12 +478,20 @@
         in_gain.reshape(2 * n_z, 1, feats),
         key_weight,
         value_weight,
-        decay_down,
+        decay_down.T,
         decay_up,
         decay_bias.reshape(1, -1),
         new_query,
-        out_gain.reshape(1, -1),
     )
+    return pl.pallas_call(
+        norm_kernel,
+        out_shape=(
+            jax.ShapeDtypeStruct((seqs, heads, share, DV), BF16),
+            jax.ShapeDtypeStruct((seqs, heads * DV), BF16),
+        ),
+        in_specs=[vmem, vmem, vmem],
+        out_specs=(vmem, vmem),
+    )(cache, parts, out_gain.reshape(1, -1))
 
 
 def solution(mesh):

time: 101 us -> 106 us (1.050)
  Pallas kernels: 94.7 us -> 105 us
  local copies, waits for them, and re-layouts: 5.02 us -> 0 us
    pallas_call x1, Pallas kernels: 94.7 us -> 103 us  [per_device(): pl.pallas_call(functools.partial(kernel, n_sp, n_z), out_shape=(jax.Shape...]
    unnamed x3 -> x0, local copies, waits for them, and re-layouts: 5.02 us -> none
    pallas_call x0 -> x1, Pallas kernels: none -> 1.55 us  [per_device(): pl.pallas_call(norm_kernel, out_shape=(jax.ShapeDtypeStruct((seqs, heads,...]
where the time goes in v2:
time: 106 us
  Pallas kernels  105 us (99%)
    pallas_call x1, Pallas kernels, per_device(): pl.pallas_call(functools.partial(kernel, n_sp, n_z), out_shape=(jax.Shape...  103 us

profile of v2, /device:TPU:0, one launch (start us, length us, event | category | flops | bytes accessed | tf_op | source)
XLA Modules:
  0.0 105.7 jit_solution(7040532318048600557)
XLA Ops:
  0.6 103.5 %shard_map.104 = (bf16[2,2,32,256]{3,2,1,0:T(8,128)(2,1)}, f32[2,4,2,256]{3,2,1,0:T(2,128)}) custom-call(bf16[2,512,512]{2,1,0:T(8,128)(2,1)} %x_ref.1, f32[8,1,512]{2,1,0:T(1,128)} %bitcast.5, bf16[4096,256]{1,0:T(8,128)(2,1)} %wk_hbm.1, bf16[4096,512]{1,0:T(8,128)(2,1)} %wv_hbm.1, bf16[32,4096]{1,0:T(8,128)(2,1)} %bitcast.4, bf16[32,2048]{1,0:T(8,128)(2,1)} %up_hbm.1, ...), custom_call_target="tpu_custom_call" | custom-call | tf_op jit(solution)/shard_map/pallas_call | solution.py:436
  104.1 1.5 %shard_map.105 = (bf16[2,2,32,256]{3,2,1,0:T(8,128)(2,1)}, bf16[2,512]{1,0:T(2,128)(2,1)}) custom-call(bf16[2,2,32,256]{3,2,1,0:T(8,128)(2,1)} %get-tuple-element.4.cache_in, f32[2,4,2,256]{3,2,1,0:T(2,128)} %get-tuple-element.5.parts_ref, f32[1,256]{1,0:T(1,128)} %bitcast.7), custom_call_target="tpu_custom_call" | custom-call | tf_op jit(solution)/shard_map/pallas_call | solution.py:486

commit v3 on v2

--- a/solution.py
+++ b/solution.py
@@ -9,8 +9,8 @@
 
 DK = 128
 DV = 256
-CHUNK = 128
-AHEAD = 4
+CHUNK = 256
+AHEAD = 2
 MESH = pl.DeviceIdType.MESH
 F32 = jnp.float32
 BF16 = jnp.bfloat16
@@ -28,13 +28,13 @@
     n_sp,
     n_z,
     x_ref,
-    gain_ref,
+    gain_hbm,
     wk_hbm,
     wv_hbm,
     wd_hbm,
     up_hbm,
     bias_hbm,
-    query_ref,
+    query_hbm,
     cache_ref,
     parts_ref,
     xbuf,
@@ -43,6 +43,8 @@
     wd,
     up,
     bias,
+    gain_ref,
+    query_ref,
     acc_k,
     acc_v,
     acc_l,
@@ -56,6 +58,7 @@
     load_sem,
     own_sem,
     line_send,
+    relay_send,
     pair_send,
     recv,
     tot_send,
@@ -84,6 +87,8 @@
         pltpu.make_async_copy(wd_hbm, wd, load_sem.at[2]),
         pltpu.make_async_copy(up_hbm.at[:, pl.ds(first, key_cols)], up, load_sem.at[3]),
         pltpu.make_async_copy(bias_hbm.at[:, pl.ds(first, key_cols)], bias, load_sem.at[4]),
+        pltpu.make_async_copy(gain_hbm, gain_ref, load_sem.at[5]),
+        pltpu.make_async_copy(query_hbm, query_ref, load_sem.at[6]),
     ]
 
     def chunk_rows(j):
@@ -97,15 +102,49 @@
             x_ref.at[seq, pl.ds(start, CHUNK), :], xbuf.at[j, z, c], own_sem.at[j]
         )
 
-    def line_copy(j, zz, way):
+    def line_copy(j, there):
+        return pltpu.make_async_remote_copy(
+            src_ref=xbuf.at[j, z, c],
+            dst_ref=xbuf.at[j, z, c],
+            send_sem=line_send.at[j, there],
+            recv_sem=recv.at[j, z, c],
+            device_id={"tp": there * 2 + c},
+            device_id_type=MESH,
+        )
+
+    def relay_copy(j, zz, end):
         return pltpu.make_async_remote_copy(
             src_ref=xbuf.at[j, zz, c],
             dst_ref=xbuf.at[j, zz, c],
-            send_sem=line_send.at[(way + 1) // 2, j, zz],
+            send_sem=relay_send.at[j, zz],
             recv_sem=recv.at[j, zz, c],
-            device_id={"tp": tp + 2 * way},
+            device_id={"tp": end * 2 + c},
             device_id_type=MESH,
         )
+
+    ends = ((0, 1), (n_z - 1, n_z - 2))
+
+    def each_end(act):
+        for end, inner in ends:
+
+            @pl.when(z == inner)
+            def _():
+                act(end)
+
+    def each_inner(act):
+        for there in range(1, n_z - 1):
+
+            @pl.when(z != there)
+            def _():
+                act(there)
+
+    def each_relayed(zz, act):
+        for end, inner in ends:
+            beyond = zz > inner if end == 0 else zz < inner
+
+            @pl.when((z == inner) & beyond)
+            def _():
+                act(end)
 
     def pair_copy(j, zz, cc):
         return pltpu.make_async_remote_copy(
@@ -119,15 +158,20 @@
 
     for j in range(chunks):
         own_copy(j).start()
+    for load in loads:
+        load.start()
 
     barrier = pltpu.get_barrier_semaphore()
-    for way in (-1, 1):
-        there = z + way
-
-        @pl.when((there >= 0) & (there < n_z))
+    at_end = (z == 0) | (z == n_z - 1)
+    for there in range(n_z):
+        met = z != there
+        if n_z > 2 and there in (0, n_z - 1):
+            met = met & jnp.logical_not(at_end)
+
+        @pl.when(met)
         def _():
             pl.semaphore_signal(
-                barrier, inc=1, device_id={"tp": tp + 2 * way}, device_id_type=MESH
+                barrier, inc=1, device_id={"tp": there * 2 + c}, device_id_type=MESH
             )
 
     pl.semaphore_signal(barrier, inc=1, device_id={"tp": tp + 1 - 2 * c}, device_id_type=MESH)
@@ -135,24 +179,18 @@
         pl.semaphore_signal(
             barrier, inc=1, device_id={"sp": lax.rem(sp + off, n_sp)}, device_id_type=MESH
         )
-    lines = jnp.where(z > 0, 1, 0) + jnp.where(z < n_z - 1, 1, 0)
-    pl.semaphore_wait(barrier, lines + n_sp)
-
-    def send_own(j):
+    far = jnp.where(at_end, 1, 0) if n_z > 2 else 0
+    pl.semaphore_wait(barrier, n_z - 1 + n_sp - far)
+
+    def send_end(j):
+        each_end(lambda end: line_copy(j, end).start())
+
+    for j in range(chunks):
         own_copy(j).wait()
-        for way in (-1, 1):
-            there = z + way
-
-            @pl.when((there >= 0) & (there < n_z))
-            def _():
-                line_copy(j, z, way).start()
-
+        each_inner(lambda there: line_copy(j, there).start())
+        if j < AHEAD:
+            send_end(j)
         pair_copy(j, z, c).start()
-
-    for j in range(min(AHEAD, chunks)):
-        send_own(j)
-    for load in loads:
-        load.start()
     for load in loads:
         load.wait()
 
@@ -187,13 +225,8 @@
         def _():
             @pl.when(i > 0)
             def _():
-                line_copy(j, zz, 1).wait_recv()
-                onward = z - way
-
-                @pl.when((onward >= 0) & (onward < n_z))
-                def _():
-                    line_copy(j, zz, -way).start()
-
+                relay_copy(j, zz, 0).wait_recv()
+                each_relayed(zz, lambda end: relay_copy(j, zz, end).start())
                 pair_copy(j, zz, c).start()
 
             add_shard(j, zz, c)
@@ -338,10 +371,30 @@
             read_copy(seq, peer, peer).wait_recv()
         parts_ref[seq] = reads[seq]
 
+    def drain(j, _):
+        pair_copy(j, z, c).wait_send()
+        each_inner(lambda there: line_copy(j, there).wait_send())
+        each_end(lambda end: line_copy(j, end).wait_send())
+
+        def inner(i, _):
+            away = (i + 1) // 2
+            way = 1 - 2 * lax.rem(i, 2)
+            zz = z + way * away
+
+            @pl.when((zz >= 0) & (zz < n_z))
+            def _():
+                each_relayed(zz, lambda end: relay_copy(j, zz, end).wait_send())
+                pair_copy(j, zz, c).wait_send()
+
+            return 0
+
+        lax.fori_loop(1, 2 * n_z - 1, inner, 0)
+        return 0
+
     def chunk_step(j, _):
         @pl.when(j + AHEAD < chunks)
         def _():
-            send_own(j + AHEAD)
+            send_end(j + AHEAD)
 
         clear_chunk()
 
@@ -351,42 +404,20 @@
 
         lax.fori_loop(0, 2 * n_z - 1, inner, 0)
         finish_chunk(j)
+
+        @pl.when((j > 0) & (j < chunks - 1))
+        def _():
+            drain(j - 1, 0)
+
         return 0
 
     lax.fori_loop(0, chunks - 1, chunk_step, 0)
     for seq in range(seqs - 1):
         send_reads(seq)
     chunk_step(chunks - 1, 0)
-    def drain(j, _):
-        pair_copy(j, z, c).wait_send()
-        for way in (-1, 1):
-            there = z + way
-
-            @pl.when((there >= 0) & (there < n_z))
-            def _():
-                line_copy(j, z, way).wait_send()
-
-        def inner(i, _):
-            away = (i + 1) // 2
-            way = 1 - 2 * lax.rem(i, 2)
-            zz = z + way * away
-
-            @pl.when((zz >= 0) & (zz < n_z))
-            def _():
-                onward = z - way
-
-                @pl.when((onward >= 0) & (onward < n_z))
-                def _():
-                    line_copy(j, zz, -way).wait_send()
-
-                pair_copy(j, zz, c).wait_send()
-
-            return 0
-
-        lax.fori_loop(1, 2 * n_z - 1, inner, 0)
-        return 0
-
-    lax.fori_loop(0, chunks, drain, 0)
+    if chunks > 1:
+        drain(chunks - 2, 0)
+    drain(chunks - 1, 0)
     send_reads(seqs - 1)
     for seq in range(seqs):
         give_read(seq)
@@ -439,7 +470,7 @@
             jax.ShapeDtypeStruct((seqs, heads, share, DV), BF16),
             jax.ShapeDtypeStruct((seqs, n_sp, heads, DV), F32),
         ),
-        in_specs=[hbm, vmem, hbm, hbm, hbm, hbm, hbm, vmem],
+        in_specs=[hbm] * 8,
         out_specs=(vmem, vmem),
         scratch_shapes=[
             pltpu.VMEM((chunks, n_z, 2, CHUNK, feats), BF16),
@@ -448,6 +479,8 @@
             pltpu.VMEM((rank, model), BF16),
             pltpu.VMEM((rank, key_cols), BF16),
             pltpu.VMEM((1, key_cols), F32),
+            pltpu.VMEM((2 * n_z, 1, feats), F32),
+            pltpu.VMEM((seqs, key_cols), BF16),
             pltpu.VMEM((CHUNK, key_cols), F32),
             pltpu.VMEM((CHUNK, value_cols), F32),
             pltpu.VMEM((CHUNK, rank), F32),
@@ -458,9 +491,10 @@
             pltpu.VMEM((seqs, n_sp, heads, share, DV), BF16),
             pltpu.VMEM((seqs, n_sp, heads, share, DV), BF16),
             pltpu.VMEM((seqs, n_sp, heads, DV), F32),
-            dma((5,)),
+            dma((7,)),
             dma((chunks,)),
-            dma((2, chunks, n_z)),
+            dma((chunks, n_z)),
+            dma((chunks, n_z)),
             dma((chunks, n_z)),
             dma((chunks, n_z, 2)),
             dma((seqs, n_sp)),

time: 106 us -> 87.6 us (0.83)
  Pallas kernels: 105 us -> 86.8 us
    pallas_call x1, Pallas kernels: 103 us -> 85.3 us  [per_device(): pl.pallas_call(functools.partial(kernel, n_sp, n_z), out_shape=(jax.Shape...]
where the time goes in v3:
time: 87.6 us; the launch traced here: 87.5 us
  Pallas kernels  86.8 us (99%)
    pallas_call x1, Pallas kernels, per_device(): pl.pallas_call(functools.partial(kernel, n_sp, n_z), out_shape=(jax.Shape...  85.3 us

profile of v3, /device:TPU:0, one launch (start us, length us, event | category | flops | bytes accessed | tf_op | source)
XLA Modules:
  0.0 87.5 jit_solution(2909430459953213127)
XLA Ops:
  0.6 85.3 %shard_map.104 = (bf16[2,2,32,256]{3,2,1,0:T(8,128)(2,1)}, f32[2,4,2,256]{3,2,1,0:T(2,128)}) custom-call(bf16[2,512,512]{2,1,0:T(8,128)(2,1)} %x_ref.1, f32[8,1,512]{2,1,0:T(1,128)} %bitcast.5, bf16[4096,256]{1,0:T(8,128)(2,1)} %wk_hbm.1, bf16[4096,512]{1,0:T(8,128)(2,1)} %wv_hbm.1, bf16[32,4096]{1,0:T(8,128)(2,1)} %bitcast.4, bf16[32,2048]{1,0:T(8,128)(2,1)} %up_hbm.1, ...), custom_call_target="tpu_custom_call" | custom-call | tf_op jit(solution)/shard_map/pallas_call | solution.py:467
  85.9 1.5 %shard_map.105 = (bf16[2,2,32,256]{3,2,1,0:T(8,128)(2,1)}, bf16[2,512]{1,0:T(2,128)(2,1)}) custom-call(bf16[2,2,32,256]{3,2,1,0:T(8,128)(2,1)} %get-tuple-element.4.cache_in, f32[2,4,2,256]{3,2,1,0:T(2,128)} %get-tuple-element.5.parts_ref, f32[1,256]{1,0:T(1,128)} %bitcast.7), custom_call_target="tpu_custom_call" | custom-call | tf_op jit(solution)/shard_map/pallas_call | solution.py:520

commit v4 on v3

--- a/solution.py
+++ b/solution.py
@@ -243,23 +243,21 @@
 
         inv_rms = lax.rsqrt(jnp.sum(acc_s[...], axis=1, keepdims=True) / model + 1e-06)
         low_rank = acc_l[...] * inv_rms
-        gate = (
-            jnp.dot(
-                low_rank,
-                up[...].astype(F32),
-                precision=lax.Precision.HIGHEST,
-                preferred_element_type=F32,
-            )
-            + bias[...]
+        gate = bias[...] + jnp.dot(
+            jnp.concatenate(split3(low_rank), axis=1),
+            jnp.concatenate([up[...]] * 3, axis=0),
+            preferred_element_type=F32,
         )
         log_decay = (jnp.minimum(gate, 0.0) - jnp.log1p(jnp.exp(-jnp.abs(gate)))) / 16.0
         later = (
             lax.broadcasted_iota(jnp.int32, (CHUNK, CHUNK), 1)
             > lax.broadcasted_iota(jnp.int32, (CHUNK, CHUNK), 0)
         ).astype(BF16)
-        suffix = carry[...]
-        for piece in split3(log_decay):
-            suffix = suffix + jnp.dot(later, piece, preferred_element_type=F32)
+        suffix = carry[...] + jnp.dot(
+            jnp.concatenate([later] * 3, axis=1),
+            jnp.concatenate(split3(log_decay), axis=0),
+            preferred_element_type=F32,
+        )
         carry[...] = carry[...] + jnp.sum(log_decay, axis=0, keepdims=True)
         last = lax.rem(j, per_seq) == per_seq - 1
 

time: 87.6 us -> 87.4 us (level)
  no operation moved by 1% of the time
where the time goes in v4:
time: 87.4 us; the launch traced here: 87.2 us
  Pallas kernels  86.6 us (99%)
    pallas_call x1, Pallas kernels, per_device(): pl.pallas_call(functools.partial(kernel, n_sp, n_z), out_shape=(jax.Shape...  85.1 us

profile of v4, /device:TPU:0, one launch (start us, length us, event | category | flops | bytes accessed | tf_op | source)
XLA Modules:
  0.0 87.2 jit_solution(438994898594504486)
XLA Ops:
  0.6 85.1 %shard_map.104 = (bf16[2,2,32,256]{3,2,1,0:T(8,128)(2,1)}, f32[2,4,2,256]{3,2,1,0:T(2,128)}) custom-call(bf16[2,512,512]{2,1,0:T(8,128)(2,1)} %x_ref.1, f32[8,1,512]{2,1,0:T(1,128)} %bitcast.5, bf16[4096,256]{1,0:T(8,128)(2,1)} %wk_hbm.1, bf16[4096,512]{1,0:T(8,128)(2,1)} %wv_hbm.1, bf16[32,4096]{1,0:T(8,128)(2,1)} %bitcast.4, bf16[32,2048]{1,0:T(8,128)(2,1)} %up_hbm.1, ...), custom_call_target="tpu_custom_call" | custom-call | tf_op jit(solution)/shard_map/pallas_call | solution.py:465
  85.7 1.5 %shard_map.105 = (bf16[2,2,32,256]{3,2,1,0:T(8,128)(2,1)}, bf16[2,512]{1,0:T(2,128)(2,1)}) custom-call(bf16[2,2,32,256]{3,2,1,0:T(8,128)(2,1)} %get-tuple-element.4.cache_in, f32[2,4,2,256]{3,2,1,0:T(2,128)} %get-tuple-element.5.parts_ref, f32[1,256]{1,0:T(1,128)} %bitcast.7), custom_call_target="tpu_custom_call" | custom-call | tf_op jit(solution)/shard_map/pallas_call | solution.py:518
